TPU v7x, 32 devices: a whole 2x2x4 slice. The times are simulated.
32 devices in a mesh: sp: 8 (over z, x), tp: 4 (over y, core).
Axes of the slice: x: 2, y: 2, z: 4, core: 2. Of those that a mesh axis runs over, the one named last changes fastest.
Arguments:
- queries_one: bfloat16 [1024, 2048], P('sp', 'tp'), may hold values from -6.2 to 6.2
- keys_one: bfloat16 [1024, 2048], P('sp', 'tp'), may hold values from -5 to 5
- values_one: bfloat16 [1024, 2048], P('sp', 'tp'), may hold values from -6 to 6
- queries_two: bfloat16 [1024, 1024], P('sp', 'tp'), may hold values from -6.2 to 6.2
- keys_two: bfloat16 [1024, 1024], P('sp', 'tp'), may hold values from -5 to 5
- values_two: bfloat16 [1024, 1024], P('sp', 'tp'), may hold values from -6 to 6
- key_offset: bfloat16 [1024, 2, 16], P('sp', None, 'tp'), may hold values from -14 to 0
- out_one: bfloat16 [2048, 4096], P('tp'), may hold values from -0.109375 to 0.109375
- out_two: bfloat16 [1024, 4096], P('tp'), may hold values from -0.109375 to 0.109375
- residual: bfloat16 [1024, 4096], P('sp', 'tp'), may hold values from -6 to 6
- norm_gain: float32 [4096], replicated, may hold values from 0.1 to 1.9
- routes: int32 [1024, 2], P('sp'), may hold values from 0 to 7, all different within a row; in each aligned block of 128 rows (0 to 127, 128 to 255, ...) at most 64 rows name the same one
- route_weight: float32 [1024, 2], P('sp'), may hold values from 0.2 to 1
- expert_gate: bfloat16 [8, 4096, 2048], P('sp', None, 'tp'), may hold values from -0.09375 to 0.09375
- expert_up: bfloat16 [8, 4096, 2048], P('sp', None, 'tp'), may hold values from -0.09375 to 0.09375
- expert_down: bfloat16 [8, 2048, 4096], P('sp', None, 'tp'), may hold values from -0.125 to 0.125
Outputs:
- mixed: bfloat16 [1024, 4096], P('sp', 'tp')
Inputs may be any that keep to these rules, and one draw needn't show every extreme that they name: `routes`: each row names two different experts; in each aligned block of 128 rows no expert is named more than 64 times, a bound that some block reaches.
All inputs are finite; a program needn't handle non-finite values.
Results may differ from a plain program's by a relative error of at most 0.015.
Values may be sent and summed in bfloat16 or wider, within the bound.
No kernel may reach another device: no remote copies, remote signals or barrier semaphores. Data moves between devices by JAX's collectives and lax.ppermute only.
A program may use at most 64 MiB of HBM per device.

v0:
```python
import jax
import jax.numpy as jnp
from jax import lax
from jax.sharding import PartitionSpec as P

DH1 = 128
DH2 = 64
EPS = 1e-06


def stick_group(query, keys, values, offset, head_size, own_start, key_block):
    row_count = query.shape[0]
    head_count = query.shape[1] // head_size
    query_heads = query.reshape(row_count, head_count, head_size)
    query_pos = own_start + jnp.arange(row_count, dtype=jnp.int32)
    block_count = (own_start + row_count + key_block - 1) // key_block

    def key_step(step_index, state_pair):
        summed, carried = state_pair
        first_key = (block_count - 1 - step_index) * key_block
        key_rows = lax.dynamic_slice_in_dim(keys, first_key, key_block, 0).reshape(
            key_block, head_count, head_size
        )
        value_rows = lax.dynamic_slice_in_dim(values, first_key, key_block, 0).reshape(
            key_block, head_count, head_size
        )
        bias_rows = lax.dynamic_slice_in_dim(offset, first_key, key_block, 0).astype(jnp.float32)
        scores = jnp.einsum(
            "qhd,khd->hqk", query_heads, key_rows, preferred_element_type=jnp.float32
        )
        scores = scores * head_size ** (-0.5) + bias_rows.T[:, None, :]
        key_pos = first_key + jnp.arange(key_block, dtype=jnp.int32)
        causal = key_pos[None, :] < query_pos[:, None]
        log_beta = jax.nn.log_sigmoid(scores)
        log_rest = jnp.where(causal, jax.nn.log_sigmoid(-scores), 0.0)
        shifted = jnp.pad(log_rest[..., 1:], ((0, 0), (0, 0), (0, 1)))
        within = lax.cumsum(shifted, axis=2, reverse=True)
        weights = jnp.where(causal, jnp.exp(log_beta + within + carried[..., None]), 0.0).astype(
            jnp.bfloat16
        )
        summed = summed + jnp.einsum(
            "hqk,khd->hqd", weights, value_rows, preferred_element_type=jnp.float32
        )
        carried = carried + jnp.sum(log_rest, axis=2)
        return (summed, carried)

    start_state = (
        jnp.zeros((head_count, row_count, head_size), jnp.float32),
        jnp.zeros((head_count, row_count), jnp.float32),
    )
    summed, _ = lax.fori_loop(0, block_count, key_step, start_state)
    return summed.transpose(1, 0, 2).reshape(row_count, head_count * head_size).astype(jnp.bfloat16)


def body(
    queries_one,
    keys_one,
    values_one,
    queries_two,
    keys_two,
    values_two,
    key_offset,
    out_one,
    out_two,
    residual,
    norm_gain,
    routes,
    route_weight,
    expert_gate,
    expert_up,
    expert_down,
):
    row_count = queries_one.shape[0]
    spread = lax.axis_size("sp")
    tp_count = lax.axis_size("tp")
    own_start = lax.axis_index("sp") * row_count
    factor = max(1, min(spread, 512 // row_count))
    while spread % factor:
        factor -= 1
    key_block = row_count * factor
    far_k1, far_v1, far_k2, far_v2, far_offset = (
        lax.all_gather(keys_one, "sp", axis=0, tiled=True),
        lax.all_gather(values_one, "sp", axis=0, tiled=True),
        lax.all_gather(keys_two, "sp", axis=0, tiled=True),
        lax.all_gather(values_two, "sp", axis=0, tiled=True),
        lax.all_gather(key_offset, "sp", axis=0, tiled=True),
    )
    attended_one = stick_group(
        queries_one, far_k1, far_v1, far_offset[:, 0, :], DH1, own_start, key_block
    )
    attended_two = stick_group(
        queries_two, far_k2, far_v2, far_offset[:, 1, :], DH2, own_start, key_block
    )
    partial_value = jnp.dot(attended_one, out_one, preferred_element_type=jnp.float32)
    partial_value = partial_value + jnp.dot(
        attended_two, out_two, preferred_element_type=jnp.float32
    )
    columns = residual.shape[1]
    column_start = lax.axis_index("tp") * columns
    resid_full = lax.all_gather(residual, "tp", axis=1, tiled=True)
    projected = lax.psum(partial_value.astype(jnp.bfloat16), "tp").astype(jnp.float32)
    stream = (resid_full.astype(jnp.float32) + projected).astype(jnp.bfloat16)
    stream_f = stream.astype(jnp.float32)
    normed = (
        stream_f * lax.rsqrt(jnp.mean(stream_f * stream_f, axis=1, keepdims=True) + EPS) * norm_gain
    ).astype(jnp.bfloat16)
    stream_own = lax.dynamic_slice_in_dim(stream, column_start, columns, 1)
    capacity = tp_count * ((4 * row_count // spread + tp_count - 1) // tp_count)
    flat_ids = routes.reshape(-1)
    onehot = (flat_ids[:, None] == jnp.arange(spread, dtype=jnp.int32)[None, :]).astype(jnp.int32)
    before = jnp.cumsum(onehot, axis=0) - onehot
    slot_of = flat_ids * capacity + jnp.sum(before * onehot, axis=1)
    chosen = slot_of[:, None] == jnp.arange(spread * capacity, dtype=jnp.int32)[None, :]
    selector = jnp.any(chosen.reshape(row_count, 2, spread * capacity), axis=1).T.astype(
        jnp.bfloat16
    )
    outgoing = jnp.dot(selector, normed, preferred_element_type=jnp.float32).astype(jnp.bfloat16)
    outgoing = outgoing.reshape(spread, capacity, normed.shape[1])
    gate_w = expert_gate[0]
    up_w = expert_up[0]
    down_w = expert_down[0]
    share_size = capacity // tp_count
    own_part = lax.dynamic_slice_in_dim(outgoing, lax.axis_index("tp") * share_size, share_size, 1)
    arrived = lax.all_to_all(own_part, "sp", split_axis=0, concat_axis=0, tiled=True)
    arrived = lax.all_gather(arrived, "tp", axis=1, tiled=True)
    sources, items, _ = arrived.shape
    flat_rows = arrived.reshape(sources * items, arrived.shape[2])
    gate_act = jnp.dot(flat_rows, gate_w, preferred_element_type=jnp.float32)
    up_act = jnp.dot(flat_rows, up_w, preferred_element_type=jnp.float32)
    hidden = (jax.nn.silu(gate_act) * up_act).astype(jnp.bfloat16)
    summed = jnp.dot(
        lax.all_gather(hidden, "tp", axis=1, tiled=True), down_w, preferred_element_type=jnp.float32
    )
    returned = lax.all_to_all(
        summed.astype(jnp.bfloat16).reshape(sources, items, down_w.shape[1]),
        "sp",
        split_axis=0,
        concat_axis=0,
        tiled=True,
    )
    back_rows = returned.reshape(spread * capacity, returned.shape[2])
    picked = jnp.dot(chosen.astype(jnp.bfloat16), back_rows, preferred_element_type=jnp.float32)
    picked = picked.reshape(row_count, 2, back_rows.shape[1])
    combined = route_weight[:, 0:1] * picked[:, 0] + route_weight[:, 1:2] * picked[:, 1]
    return (stream_own.astype(jnp.float32) + combined).astype(jnp.bfloat16)


def solution(mesh):
    return jax.shard_map(
        body,
        mesh=mesh,
        in_specs=(
            P("sp", "tp"),
            P("sp", "tp"),
            P("sp", "tp"),
            P("sp", "tp"),
            P("sp", "tp"),
            P("sp", "tp"),
            P("sp", None, "tp"),
            P("tp", None),
            P("tp", None),
            P("sp", "tp"),
            P(),
            P("sp", None),
            P("sp", None),
            P("sp", None, "tp"),
            P("sp", None, "tp"),
            P("sp", None, "tp"),
        ),
        out_specs=P("sp", "tp"),
        check_vma=False,
    )
```

profile of v0, /device:TPU:0, one launch (start us, length us, event | category | flops | bytes accessed | tf_op | source)
XLA Modules:
  0.0 333.9 jit_solution(7751054359413685680)
XLA Ops:
  6.5 1.8 copy.80
  8.4 1.7 copy.78
  10.2 0.7 all-gather.6.cloned.1.call-update
  10.9 0.8 copy.86
  12.0 22.6 %all_gather.26 = bf16[1024,2,4]{0,2,1:T(4,128)(2,1)S(1)} all-gather(bf16[128,2,4]{0,2,1:T(4,128)(2,1)} %param.26), channel_id=1, replica_groups=mesh['sp'=8,'tp'=4] {'sp'}, dimensions={0}, use_global_device_ids=true | all-gather | bytes 18432 | tf_op jit(solution)/shard_map/all_gather | solution.py:86
  34.6 1.0 copy.79
  35.6 0.8 copy.81
  36.4 1.0 copy.83
  37.4 28.0 %all_gather.28 = bf16[1024,256]{0,1:T(8,128)(2,1)S(1)} all-gather(bf16[128,256]{0,1:T(8,128)(2,1)S(1)} %copy.83), channel_id=1, replica_groups=mesh['sp'=8,'tp'=4] {'sp'}, dimensions={0}, use_global_device_ids=true | all-gather | bytes 589824 | tf_op jit(solution)/shard_map/all_gather | solution.py:84
  65.3 0.9 copy.85
  66.3 28.3 %all_gather.29 = bf16[1024,256]{0,1:T(8,128)(2,1)S(1)} all-gather(bf16[128,256]{0,1:T(8,128)(2,1)S(1)} %copy.85), channel_id=1, replica_groups=mesh['sp'=8,'tp'=4] {'sp'}, dimensions={0}, use_global_device_ids=true | all-gather | bytes 589824 | tf_op jit(solution)/shard_map/all_gather | solution.py:85
  94.5 1.6 copy.84
  96.1 0.7 broadcast_in_dim.40
  96.8 11.1 %while.31 = (s32[]{:T(128)}, f32[4,128,64]{1,2,0:T(8,128)}, f32[4,128]{1,0:T(4,128)S(1)}, s32[]{:T(128)}, s32[]{:T(128)}, /*index=5*/bf16[1024,256]{0,1:T(8,128)...) while((s32[]{:T(128)}, f32[4,128,64]{1,2,0:T(8,128)}, ...), condition=%wide.region_9.10_spmd.clone, body=%wide.region_5.9_spmd.clone.sunk | while | flops 106801288 | bytes 31546788 | solution.py:51
  97.0 2.9 fusion.114
  100.1 4.8 %fusion.115 = f32[4,128,4,128]{1,2,3,0:T(4,128)S(1)} fusion(f32[4,128,4,128]{1,3,2,0:T(8,128)S(1)} %bitcast.143), kind=kOutput, calls=%fused_computation.40.clone.1 | output fusion | flops 33292288 | bytes 2097152 | tf_op jit(solution)/shard_map/reduce-window.16
  104.9 0.2 broadcast_add_fusion.5
  105.3 0.9 copy-done.2
  106.1 0.8 fusion.116
  107.0 0.2 convolution_add_fusion.6
  107.2 0.7 copy-done.9
  107.9 1.6 convert_element_type.91
  109.5 0.6 reduce-window.42
  110.1 12.8 %while.30 = (s32[]{:T(128)}, f32[4,128,128]{2,1,0:T(8,128)S(1)}, f32[4,128]{1,0:T(4,128)S(1)}, s32[]{:T(128)}, s32[]{:T(128)}, /*index=5*/bf16[1024,512]{0,1:T(8...) while((s32[]{:T(128)}, f32[4,128,128]{2,1,0:T(8,128)S(1)}, ...), condition=%wide.region_4.5_spmd.clone, body=%wide.region_0.4_spmd.clone.sunk | while | flops 173942912 | bytes 26107160 | solution.py:51
  110.3 2.1 constant_dynamic-slice_fusion.7
  112.6 2.9 fusion.106
  115.6 4.8 %fusion.107 = f32[4,128,4,128]{1,2,3,0:T(4,128)S(1)} fusion(f32[4,128,4,128]{1,3,2,0:T(8,128)S(1)} %bitcast.144), kind=kOutput, calls=%fused_computation.16.clone.1 | output fusion | flops 33292288 | bytes 2097152 | tf_op jit(solution)/shard_map/reduce-window.14
  120.5 0.2 broadcast_add_fusion.4
  120.8 0.9 copy-done.3
  121.7 0.8 fusion.108
  122.5 0.4 convolution_add_fusion.5
  123.0 2.9 fusion.67
  126.0 1.5 fusion.28
  127.6 0.2 slice_reduce_fusion
  128.4 58.6 %all-reduce.4.cloned.1.call-done = bf16[128,4096]{1,0:T(8,128)(2,1)} async-done(((bf16[128,4096]{1,0:T(8,128)(2,1)}), bf16[128,4096]{1,0:T(8,128)(2,1)}) %all-reduce.4.cloned.1.call-update) | async-done | bytes 1048592 | tf_op jit(solution)/shard_map/psum | solution.py:101
  187.0 2.0 fusion.35
  189.0 1.4 convolution_convert_fusion
  190.5 30.6 %all_to_all.10 = bf16[8,16,4096]{2,1,0:T(8,128)(2,1)} all-to-all(bf16[8,16,4096]{2,1,0:T(8,128)(2,1)S(1)} %constant_dynamic-slice_fusion.4), channel_id=1, replica_groups=mesh['sp'=8,'tp'=4] {'sp'}, dimensions={0} | all-to-all | bytes 2097152 | tf_op jit(solution)/shard_map/all_to_all | solution.py:124
  221.1 0.3 all-gather.14.cloned.1.call-start
  221.4 33.2 %all-gather.12.cloned.1.call-done = bf16[8,64,4096]{2,1,0:T(8,128)(2,1)} async-done(((bf16[8,16,4096]{2,1,0:T(8,128)(2,1)}), bf16[8,64,4096]{2,1,0:T(8,128)(2,1)}) %all-gather.12.cloned.1.call-update) | async-done | bytes 4194320 | tf_op jit(solution)/shard_map/all_gather | solution.py:125
  254.6 5.9 %fusion.33 = f32[512,512]{1,0:T(8,128)S(1)} fusion(bf16[512,4096]{1,0:T(8,128)(2,1)} %bitcast.155, bf16[1,4096,512]{2,1,0:T(8,128)(2,1)} %param.33), kind=kOutput, calls=%fused_computation.57 | convolution fusion | flops 2147483648 | bytes 9437184 | tf_op jit(solution)/shard_map/dot_general | solution.py:128
  260.6 3.2 fusion.44
  263.9 22.7 %all-gather.14.cloned.1.call-done = bf16[512,2048]{1,0:T(8,128)(2,1)} async-done(((bf16[512,512]{1,0:T(8,128)(2,1)}), bf16[512,2048]{1,0:T(8,128)(2,1)}) %all-gather.14.cloned.1.call-update) | async-done | bytes 2097168 | tf_op jit(solution)/shard_map/all_gather | solution.py:132
  286.6 6.2 %fusion.38 = bf16[512,1024]{1,0:T(8,128)(2,1)} fusion(bf16[512,2048]{1,0:T(8,128)(2,1)} %all-gather.14.cloned.1.call-done, bf16[1,2048,1024]{2,1,0:T(8,128)(2,1)} %param.35), kind=kOutput, calls=%fused_computation.65 | convolution fusion | flops 2148007936 | bytes 7340032 | tf_op jit(solution)/shard_map/dot_general | solution.py:131
  292.7 5.5 %all-to-all-start.1 = ((bf16[8,64,1024]{2,1,0:T(8,128)(2,1)}), bf16[8,64,1024]{2,1,0:T(8,128)(2,1)}, u32[]{:S(2)}, u32[]{:S(2)}) async-start(bf16[8,64,1024]{2,1,0:T(8,128)(2,1)} %bitcast.150), calls=%async_computation.1 | async-start | bytes 2097152 | tf_op jit(solution)/shard_map/all_to_all | solution.py:134
  298.2 26.2 %all-to-all-done.1 = bf16[8,64,1024]{2,1,0:T(8,128)(2,1)} async-done(((bf16[8,64,1024]{2,1,0:T(8,128)(2,1)}), bf16[8,64,1024]{2,1,0:T(8,128)(2,1)}, u32[]{:S(2)}, u32[]{:S(2)}) %all-to-all-start.1) | async-done | bytes 1048608 | tf_op jit(solution)/shard_map/all_to_all | solution.py:134
  324.5 1.7 fusion.56
  326.2 0.9 fusion.53
  (83 shorter events, 2.3 us)
Async XLA Ops:
  6.5 119.5 %copy-start = (bf16[256,4096]{1,0:T(8,128)(2,1)S(1)}, bf16[256,4096]{1,0:T(8,128)(2,1)}, u32[]{:S(2)}) copy-start(bf16[256,4096]{1,0:T(8,128)(2,1)} %param.28) | copy-start | bytes 6291460
  6.5 103.5 %all-gather.10.cloned.1.call-start = ((), (), s32[]{:S(2)}) async-start(), calls=%async_computation.4 | async-start | bytes 1179648 | tf_op jit(solution)/shard_map/all_gather | solution.py:83
  8.4 101.7 %all-gather.8.cloned.1.call-start = ((), (), s32[]{:S(2)}) async-start(), calls=%async_computation.3 | async-start | bytes 1179648 | tf_op jit(solution)/shard_map/all_gather | solution.py:82
  10.1 118.2 %all-gather.6.cloned.1.call-start = ((), (), s32[]{:S(2)}) async-start(), calls=%async_computation.2 | async-start | bytes 1310720 | tf_op jit(solution)/shard_map/all_gather | solution.py:100
  10.9 176.1 %all-reduce.4.cloned.1.call-start = ((), (), s32[]{:S(2)}) async-start(), calls=%async_computation.5 | async-start | bytes 2097152 | tf_op jit(solution)/shard_map/psum | solution.py:101
  96.8 3.2 copy-start.4
  96.8 3.3 copy-start.6
  104.9 1.2 copy-start.2
  104.9 2.1 copy-start.8
  105.1 2.8 copy-start.5
  105.1 2.8 copy-start.7
  107.2 0.7 copy-start.9
  120.4 1.2 copy-start.3
  120.4 2.1 copy-start.1
  122.9 3.1 copy-start.10
  126.0 2.2 copy-start.12
  126.0 63.0 %copy-start.11 = (f32[4096]{0:T(1024)S(1)}, f32[4096]{0:T(1024)}, u32[]{:S(2)}) copy-start(f32[4096]{0:T(1024)} %param.30) | copy-start | bytes 49156
  127.6 127.1 %all-gather.12.cloned.1.call-start = ((), (), s32[]{:S(2)}) async-start(), calls=%async_computation.6 | async-start | bytes 5242880 | tf_op jit(solution)/shard_map/all_gather | solution.py:125
  221.1 65.4 %all-gather.14.cloned.1.call-start = ((), (), s32[]{:S(2)}) async-start(), calls=%async_computation.7 | async-start | bytes 2621440 | tf_op jit(solution)/shard_map/all_gather | solution.py:132
  254.6 5.9 %copy-start.14 = (bf16[1,4096,512]{2,1,0:T(8,128)(2,1)S(1)}, bf16[1,4096,512]{2,1,0:T(8,128)(2,1)}, u32[]{:S(2)}) copy-start(bf16[1,4096,512]{2,1,0:T(8,128)(2,1)} %param.34) | copy-start | bytes 12582916
  254.6 5.9 %copy-start.15 = (bf16[8,64,4096]{2,1,0:T(8,128)(2,1)S(1)}, bf16[8,64,4096]{2,1,0:T(8,128)(2,1)}, u32[]{:S(2)}) copy-start(bf16[8,64,4096]{2,1,0:T(8,128)(2,1)} %all-gather.12.cloned.1.call-done) | copy-start | bytes 12582916
  263.8 34.4 %copy-start.13 = (f32[128,2]{0,1:T(2,128)S(1)}, f32[128,2]{0,1:T(2,128)}, u32[]{:S(2)}) copy-start(f32[128,2]{0,1:T(2,128)} %param.32) | copy-start | bytes 3076
  292.7 31.8 %all-to-all-start.1 = ((bf16[8,64,1024]{2,1,0:T(8,128)(2,1)}), bf16[8,64,1024]{2,1,0:T(8,128)(2,1)}, u32[]{:S(2)}, u32[]{:S(2)}) async-start(bf16[8,64,1024]{2,1,0:T(8,128)(2,1)} %bitcast.150), calls=%async_computation.1 | async-start | bytes 2097152 | tf_op jit(solution)/shard_map/all_to_all | solution.py:134
Sparse Core Ops, SparseCore 0:
  9.4 43.6 all-gather.9
  55.1 43.9 all-gather.7
  100.7 16.6 all-gather.5
  127.7 59.2 all-reduce.3
  221.3 33.3 all-gather.11
  264.0 22.5 all-gather.13
where the time goes:
time: 335 us; the launch traced here: 334 us
  waiting for transfers between devices  142 us (42%)
  blocking collectives  109 us (33%)
  matrix products  29.2 us (9%)
  other arithmetic  17.3 us (5%)
  local copies, waits for them, and re-layouts  16.3 us (5%)
  between operations  13.7 us (4%)
  starting transfers between devices  5.94 us (2%)
    psum x1, waiting for transfers between devices, body(): lax.psum(partial_value.astype(jnp.bfloat16), 'tp').astype(jnp.float32)  58.6 us
    all_gather x1, waiting for transfers between devices, body(): arrived = lax.all_gather(arrived, 'tp', axis=1, tiled=True)  33.2 us
    all_to_all x1, blocking collectives, body(): lax.all_to_all(own_part, 'sp', split_axis=0, concat_axis=0, tiled=True)  30.6 us
    all_gather x1, blocking collectives, body(): lax.all_gather(values_two, 'sp', axis=0, tiled=True)  28.3 us
    all_gather x1, blocking collectives, body(): lax.all_gather(keys_two, 'sp', axis=0, tiled=True)  28 us
    all_to_all x1, waiting for transfers between devices, body(): lax.all_to_all(summed.astype(jnp.bfloat16).reshape(sources, items, down_w...  26.2 us
    all_gather x1, waiting for transfers between devices, body(): lax.all_gather(hidden, 'tp', axis=1, tiled=True)  22.7 us
    all_gather x1, blocking collectives, body(): lax.all_gather(key_offset, 'sp', axis=0, tiled=True)  22.6 us
  transfers between devices with their start and end apart: 7, of which 4 were waited for; matrix products, arithmetic and copies ran while one was open for 11% of the time, Pallas kernels for 0%

commit v1 on v0

--- a/solution.py
+++ b/solution.py
@@ -98,7 +98,9 @@
     columns = residual.shape[1]
     column_start = lax.axis_index("tp") * columns
     resid_full = lax.all_gather(residual, "tp", axis=1, tiled=True)
-    projected = lax.psum(partial_value.astype(jnp.bfloat16), "tp").astype(jnp.float32)
+    projected = jnp.sum(lax.all_gather(partial_value.astype(jnp.bfloat16), "tp"), axis=0).astype(
+        jnp.float32
+    )
     stream = (resid_full.astype(jnp.float32) + projected).astype(jnp.bfloat16)
     stream_f = stream.astype(jnp.float32)
     normed = (

time: 335 us -> 347 us (1.036)
  waiting for transfers between devices: 142 us -> 149 us
  other arithmetic: 17.3 us -> 21.6 us
    psum x1 -> x0, waiting for transfers between devices: 58.6 us -> none  [body(): lax.psum(partial_value.astype(jnp.bfloat16), 'tp').astype(jnp.float32)]
    all_gather x0 -> x1, waiting for transfers between devices: none -> 53.3 us  [body(): lax.all_gather(partial_value.astype(jnp.bfloat16), 'tp')]
    all_gather x1, waiting for transfers between devices: 0.02 us -> 13.9 us  [body(): resid_full = lax.all_gather(residual, 'tp', axis=1, tiled=True)]
    reduce_sum x0 -> x1, other arithmetic: none -> 4.26 us  [body(): jnp.sum(lax.all_gather(partial_value.astype(jnp.bfloat16), 'tp'), axis=0)]
  transfers between devices with their start and end apart: 7 -> 7, of which waited for: 4 -> 5; matrix products, arithmetic and copies ran while one was open for 11% -> 7% of each run, Pallas kernels for 0% -> 0%
where the time goes in v1:
time: 347 us; the launch traced here: 346 us
  waiting for transfers between devices  149 us (43%)
  blocking collectives  112 us (32%)
  matrix products  28.2 us (8%)
  other arithmetic  21.6 us (6%)
  local copies, waits for them, and re-layouts  14.9 us (4%)
  between operations  13.7 us (4%)
  starting transfers between devices  5.94 us (2%)
    all_gather x1, waiting for transfers between devices, body(): lax.all_gather(partial_value.astype(jnp.bfloat16), 'tp')  53.3 us
    all_gather x1, waiting for transfers between devices, body(): arrived = lax.all_gather(arrived, 'tp', axis=1, tiled=True)  32.7 us
    all_to_all x1, blocking collectives, body(): lax.all_to_all(own_part, 'sp', split_axis=0, concat_axis=0, tiled=True)  31.5 us
    all_gather x1, blocking collectives, body(): lax.all_gather(keys_two, 'sp', axis=0, tiled=True)  29.2 us
    all_gather x1, blocking collectives, body(): lax.all_gather(values_two, 'sp', axis=0, tiled=True)  28.5 us
    all_to_all x1, waiting for transfers between devices, body(): lax.all_to_all(summed.astype(jnp.bfloat16).reshape(sources, items, down_w...  26.2 us
    all_gather x1, waiting for transfers between devices, body(): lax.all_gather(hidden, 'tp', axis=1, tiled=True)  22.7 us
    all_gather x1, blocking collectives, body(): lax.all_gather(key_offset, 'sp', axis=0, tiled=True)  22.7 us
  transfers between devices with their start and end apart: 7, of which 5 were waited for; matrix products, arithmetic and copies ran while one was open for 7% of the time, Pallas kernels for 0%

profile of v1, /device:TPU:0, one launch (start us, length us, event | category | flops | bytes accessed | tf_op | source)
XLA Modules:
  0.0 346.2 jit_solution(6327251483907981877)
XLA Ops:
  6.5 1.8 copy.78
  8.4 1.7 copy.80
  10.2 22.7 %all_gather.32 = bf16[1024,2,4]{0,2,1:T(4,128)(2,1)S(1)} all-gather(bf16[128,2,4]{0,2,1:T(4,128)(2,1)} %param.26), channel_id=1, replica_groups=mesh['sp'=8,'tp'=4] {'sp'}, dimensions={0}, use_global_device_ids=true | all-gather | bytes 18432 | tf_op jit(solution)/shard_map/all_gather | solution.py:86
  32.9 1.0 copy.83
  33.8 29.2 %all_gather.34 = bf16[1024,256]{0,1:T(8,128)(2,1)S(1)} all-gather(bf16[128,256]{0,1:T(8,128)(2,1)S(1)} %copy.83), channel_id=1, replica_groups=mesh['sp'=8,'tp'=4] {'sp'}, dimensions={0}, use_global_device_ids=true | all-gather | bytes 589824 | tf_op jit(solution)/shard_map/all_gather | solution.py:84
  63.0 1.0 copy.85
  64.0 28.5 %all_gather.35 = bf16[1024,256]{0,1:T(8,128)(2,1)S(1)} all-gather(bf16[128,256]{0,1:T(8,128)(2,1)S(1)} %copy.85), channel_id=1, replica_groups=mesh['sp'=8,'tp'=4] {'sp'}, dimensions={0}, use_global_device_ids=true | all-gather | bytes 589824 | tf_op jit(solution)/shard_map/all_gather | solution.py:85
  92.5 1.6 copy.84
  94.1 0.7 broadcast_in_dim.40
  94.7 11.1 %while.31 = (s32[]{:T(128)}, f32[4,128,64]{1,2,0:T(8,128)}, f32[4,128]{1,0:T(4,128)S(1)}, s32[]{:T(128)}, s32[]{:T(128)}, /*index=5*/bf16[1024,256]{0,1:T(8,128)...) while((s32[]{:T(128)}, f32[4,128,64]{1,2,0:T(8,128)}, ...), condition=%wide.region_9.10_spmd.clone, body=%wide.region_5.9_spmd.clone.sunk | while | flops 106801288 | bytes 31546788 | solution.py:51
  94.9 2.9 fusion.114
  98.0 4.8 %fusion.115 = f32[4,128,4,128]{1,2,3,0:T(4,128)S(1)} fusion(f32[4,128,4,128]{1,3,2,0:T(8,128)S(1)} %bitcast.144), kind=kOutput, calls=%fused_computation.40.clone.1 | output fusion | flops 33292288 | bytes 2097152 | tf_op jit(solution)/shard_map/reduce-window.16
  102.9 0.2 broadcast_add_fusion.5
  103.2 0.9 copy-done.2
  104.1 0.8 fusion.116
  104.9 0.2 convolution_add_fusion.6
  105.2 0.6 copy-done.9
  105.8 1.0 copy.79
  107.0 1.5 convert_element_type.93
  108.6 11.9 %while.30 = (s32[]{:T(128)}, f32[4,128,128]{2,1,0:T(8,128)S(1)}, f32[4,128]{1,0:T(4,128)S(1)}, s32[]{:T(128)}, s32[]{:T(128)}, /*index=5*/bf16[1024,512]{0,1:T(8...) while((s32[]{:T(128)}, f32[4,128,128]{2,1,0:T(8,128)S(1)}, ...), condition=%wide.region_4.5_spmd.clone, body=%wide.region_0.4_spmd.clone.sunk | while | flops 173942912 | bytes 27155792 | solution.py:51
  108.8 2.1 constant_dynamic-slice_fusion.7
  111.1 2.0 fusion.106
  113.2 4.8 %fusion.107 = f32[4,128,4,128]{1,2,3,0:T(4,128)S(1)} fusion(f32[4,128,4,128]{1,3,2,0:T(8,128)S(1)} %bitcast.145), kind=kOutput, calls=%fused_computation.16.clone.1 | output fusion | flops 33292288 | bytes 2097152 | tf_op jit(solution)/shard_map/reduce-window.14
  118.1 0.2 broadcast_add_fusion.4
  118.4 0.9 copy-done.3
  119.3 0.8 fusion.108
  120.1 0.4 convolution_add_fusion.5
  120.7 2.9 fusion.67
  123.6 1.5 fusion.28
  125.3 0.5 all-gather.8.cloned.1.call-update
  125.8 0.3 all-gather.14.cloned.1.call-start
  126.5 0.6 reduce-window.42
  127.1 0.2 slice_reduce_fusion
  127.8 53.3 %all-gather.18.cloned.1.call-done = bf16[512,4096]{1,0:T(8,128)(2,1)} async-done(((bf16[128,4096]{1,0:T(8,128)(2,1)}), bf16[512,4096]{1,0:T(8,128)(2,1)}) %all-gather.18.cloned.1.call-update) | async-done | bytes 4194320 | tf_op jit(solution)/shard_map/all_gather | solution.py:101
  181.0 4.3 %reduce_sum.56 = bf16[128,4096]{1,0:T(8,128)(2,1)} reduce(bf16[4,128,4096]{2,1,0:T(8,128)(2,1)} %bitcast.151, bf16[]{:T(256)} %constant.134.clone.1), dimensions={0}, to_apply=%region_10.11 | reduce | flops 1572864 | bytes 5242882 | tf_op jit(solution)/shard_map/reduce_sum | solution.py:101
  185.3 13.9 %all-gather.8.cloned.1.call-done = bf16[128,4096]{1,0:T(8,128)(2,1)} async-done(((bf16[128,1024]{1,0:T(8,128)(2,1)}), bf16[128,4096]{1,0:T(8,128)(2,1)}) %all-gather.8.cloned.1.call-update) | async-done | bytes 1048592 | tf_op jit(solution)/shard_map/all_gather | solution.py:100
  199.2 2.0 fusion.35
  201.2 1.4 convolution_convert_fusion
  202.7 31.5 %all_to_all.10 = bf16[8,16,4096]{2,1,0:T(8,128)(2,1)} all-to-all(bf16[8,16,4096]{2,1,0:T(8,128)(2,1)S(1)} %constant_dynamic-slice_fusion.4), channel_id=1, replica_groups=mesh['sp'=8,'tp'=4] {'sp'}, dimensions={0} | all-to-all | bytes 2097152 | tf_op jit(solution)/shard_map/all_to_all | solution.py:126
  234.3 32.7 %all-gather.14.cloned.1.call-done = bf16[8,64,4096]{2,1,0:T(8,128)(2,1)} async-done(((bf16[8,16,4096]{2,1,0:T(8,128)(2,1)}), bf16[8,64,4096]{2,1,0:T(8,128)(2,1)}) %all-gather.14.cloned.1.call-update) | async-done | bytes 4194320 | tf_op jit(solution)/shard_map/all_gather | solution.py:127
  266.9 5.9 %fusion.33 = f32[512,512]{1,0:T(8,128)S(1)} fusion(bf16[512,4096]{1,0:T(8,128)(2,1)} %bitcast.157, bf16[1,4096,512]{2,1,0:T(8,128)(2,1)} %param.33), kind=kOutput, calls=%fused_computation.57 | convolution fusion | flops 2147483648 | bytes 9437184 | tf_op jit(solution)/shard_map/dot_general | solution.py:130
  272.9 3.2 fusion.44
  276.2 22.7 %all-gather.16.cloned.1.call-done = bf16[512,2048]{1,0:T(8,128)(2,1)} async-done(((bf16[512,512]{1,0:T(8,128)(2,1)}), bf16[512,2048]{1,0:T(8,128)(2,1)}) %all-gather.16.cloned.1.call-update) | async-done | bytes 2097168 | tf_op jit(solution)/shard_map/all_gather | solution.py:134
  298.9 6.1 %fusion.38 = bf16[512,1024]{1,0:T(8,128)(2,1)} fusion(bf16[512,2048]{1,0:T(8,128)(2,1)} %all-gather.16.cloned.1.call-done, bf16[1,2048,1024]{2,1,0:T(8,128)(2,1)} %param.35), kind=kOutput, calls=%fused_computation.65 | convolution fusion | flops 2148007936 | bytes 7340032 | tf_op jit(solution)/shard_map/dot_general | solution.py:133
  305.0 5.5 %all-to-all-start.1 = ((bf16[8,64,1024]{2,1,0:T(8,128)(2,1)}), bf16[8,64,1024]{2,1,0:T(8,128)(2,1)}, u32[]{:S(2)}, u32[]{:S(2)}) async-start(bf16[8,64,1024]{2,1,0:T(8,128)(2,1)} %bitcast.152), calls=%async_computation.1 | async-start | bytes 2097152 | tf_op jit(solution)/shard_map/all_to_all | solution.py:136
  310.5 26.2 %all-to-all-done.1 = bf16[8,64,1024]{2,1,0:T(8,128)(2,1)} async-done(((bf16[8,64,1024]{2,1,0:T(8,128)(2,1)}), bf16[8,64,1024]{2,1,0:T(8,128)(2,1)}, u32[]{:S(2)}, u32[]{:S(2)}) %all-to-all-start.1) | async-done | bytes 1048608 | tf_op jit(solution)/shard_map/all_to_all | solution.py:136
  336.8 1.7 fusion.56
  338.5 0.9 fusion.53
  (88 shorter events, 2.5 us)
Async XLA Ops:
  6.5 117.1 %copy-start = (bf16[256,4096]{1,0:T(8,128)(2,1)S(1)}, bf16[256,4096]{1,0:T(8,128)(2,1)}, u32[]{:S(2)}) copy-start(bf16[256,4096]{1,0:T(8,128)(2,1)} %param.28) | copy-start | bytes 6291460
  6.5 102.0 %all-gather.10.cloned.1.call-start = ((), (), s32[]{:S(2)}) async-start(), calls=%async_computation.3 | async-start | bytes 1179648 | tf_op jit(solution)/shard_map/all_gather | solution.py:82
  8.4 100.2 %all-gather.12.cloned.1.call-start = ((), (), s32[]{:S(2)}) async-start(), calls=%async_computation.4 | async-start | bytes 1179648 | tf_op jit(solution)/shard_map/all_gather | solution.py:83
  10.1 170.9 %all-gather.18.cloned.1.call-start = ((), (), s32[]{:S(2)}) async-start(), calls=%async_computation.7 | async-start | bytes 5242880 | tf_op jit(solution)/shard_map/all_gather | solution.py:101
  94.7 3.2 copy-start.4
  94.7 3.2 copy-start.6
  102.8 1.2 copy-start.2
  102.8 2.1 copy-start.8
  103.1 2.8 copy-start.5
  103.1 2.8 copy-start.7
  105.1 0.7 copy-start.9
  108.8 4.3 %copy-start.11 = (bf16[128,4,128]{2,0,1:T(8,128)(2,1)}, bf16[128,4,128]{2,0,1:T(8,128)(2,1)S(1)}, u32[]{:S(2)}) copy-start(bf16[128,4,128]{2,0,1:T(8,128)(2,1)S(1)} %get-tuple-element.567) | copy-start | bytes 393220 | tf_op jit(solution)/shard_map/while
  118.0 1.2 copy-start.3
  118.1 2.1 copy-start.1
  118.3 2.2 copy-start.12
  120.5 3.1 copy-start.10
  123.6 2.4 copy-start.14
  125.2 74.0 %all-gather.8.cloned.1.call-start = ((), (), s32[]{:S(2)}) async-start(), calls=%async_computation.2 | async-start | bytes 1310720 | tf_op jit(solution)/shard_map/all_gather | solution.py:100
  125.8 141.2 %all-gather.14.cloned.1.call-start = ((), (), s32[]{:S(2)}) async-start(), calls=%async_computation.5 | async-start | bytes 5242880 | tf_op jit(solution)/shard_map/all_gather | solution.py:127
  181.0 20.2 %copy-start.13 = (f32[4096]{0:T(1024)S(1)}, f32[4096]{0:T(1024)}, u32[]{:S(2)}) copy-start(f32[4096]{0:T(1024)} %param.30) | copy-start | bytes 49156
  234.2 64.7 %all-gather.16.cloned.1.call-start = ((), (), s32[]{:S(2)}) async-start(), calls=%async_computation.6 | async-start | bytes 2621440 | tf_op jit(solution)/shard_map/all_gather | solution.py:134
  266.9 5.9 %copy-start.16 = (bf16[1,4096,512]{2,1,0:T(8,128)(2,1)S(1)}, bf16[1,4096,512]{2,1,0:T(8,128)(2,1)}, u32[]{:S(2)}) copy-start(bf16[1,4096,512]{2,1,0:T(8,128)(2,1)} %param.34) | copy-start | bytes 12582916
  266.9 5.9 %copy-start.17 = (bf16[8,64,4096]{2,1,0:T(8,128)(2,1)S(1)}, bf16[8,64,4096]{2,1,0:T(8,128)(2,1)}, u32[]{:S(2)}) copy-start(bf16[8,64,4096]{2,1,0:T(8,128)(2,1)} %all-gather.14.cloned.1.call-done) | copy-start | bytes 12582916
  276.1 34.4 %copy-start.15 = (f32[128,2]{0,1:T(2,128)S(1)}, f32[128,2]{0,1:T(2,128)}, u32[]{:S(2)}) copy-start(f32[128,2]{0,1:T(2,128)} %param.32) | copy-start | bytes 3076
  305.0 31.8 %all-to-all-start.1 = ((bf16[8,64,1024]{2,1,0:T(8,128)(2,1)}), bf16[8,64,1024]{2,1,0:T(8,128)(2,1)}, u32[]{:S(2)}, u32[]{:S(2)}) async-start(bf16[8,64,1024]{2,1,0:T(8,128)(2,1)} %bitcast.152), calls=%async_computation.1 | async-start | bytes 2097152 | tf_op jit(solution)/shard_map/all_to_all | solution.py:136
Sparse Core Ops, SparseCore 0:
  9.4 43.8 all-gather.9
  55.3 45.0 all-gather.11
  125.3 55.6 all-gather.17
  182.4 16.6 all-gather.7
  234.3 32.5 all-gather.13
  276.3 22.5 all-gather.15
